TPU v7x, 32 devices: a whole 2x2x4 slice. The times are simulated.
32 devices in a mesh: fs: 8 (over z, y), tp: 4 (over x, core).
Axes of the slice: x: 2, y: 2, z: 4, core: 2. Of those that a mesh axis runs over, the one named last changes fastest.
Arguments:
- tokens: bfloat16 [4096, 2048], P(('fs', 'tp')), may hold values from -6 to 6
- norm_one: float32 [2048], replicated, may hold values from 0.1 to 1.9
- gate_one: bfloat16 [2048, 4608], P('fs', 'tp'), may hold values from -0.125 to 0.125
- up_one: bfloat16 [2048, 4608], P('fs', 'tp'), may hold values from -0.125 to 0.125
- down_one: bfloat16 [4608, 2048], P('tp', 'fs'), may hold values from -0.1875 to 0.1875
- norm_two: float32 [2048], replicated, may hold values from 0.1 to 1.9
- gate_two: bfloat16 [2048, 4608], P('fs', 'tp'), may hold values from -0.125 to 0.125
- up_two: bfloat16 [2048, 4608], P('fs', 'tp'), may hold values from -0.125 to 0.125
- down_two: bfloat16 [4608, 2048], P('tp', 'fs'), may hold values from -0.1875 to 0.1875
Outputs:
- result: bfloat16 [4096, 2048], P(('fs', 'tp'))
All inputs are finite; a program needn't handle non-finite values.
Results may differ from a plain program's by a relative error of at most 0.015.
Values may be sent and summed in bfloat16 or wider, within the bound.
A program may use at most 64 MiB of HBM per device.

v0:
```python
import jax
import jax.numpy as jnp
from jax import lax
from jax.sharding import PartitionSpec as P

eps = 1e-06


def normalize(rows, gain):
    values = rows.astype(jnp.float32)
    scaled = values * lax.rsqrt(jnp.mean(values * values, axis=-1, keepdims=True) + eps)
    return (scaled * gain).astype(jnp.bfloat16)


def hidden_units(rows, gain, gate_w, up_w):
    normed = normalize(rows, gain)
    gate_full, up_full = (
        lax.all_gather(gate_w, "fs", axis=0, tiled=True),
        lax.all_gather(up_w, "fs", axis=0, tiled=True),
    )
    gate_sum = jnp.dot(normed, gate_full, preferred_element_type=jnp.float32)
    up_sum = jnp.dot(normed, up_full, preferred_element_type=jnp.float32)
    return (jax.nn.silu(gate_sum) * up_sum).astype(jnp.bfloat16)


def down_terms(hidden, down_w):
    return jnp.dot(
        hidden, lax.all_gather(down_w, "fs", axis=1, tiled=True), preferred_element_type=jnp.float32
    )


def on_device(tokens, norm_one, gate_one, up_one, down_one, norm_two, gate_two, up_two, down_two):
    gathered = lax.all_gather(tokens, "tp", axis=0, tiled=True)
    first_terms = down_terms(hidden_units(gathered, norm_one, gate_one, up_one), down_one)
    summed = lax.psum(first_terms.astype(jnp.bfloat16), "tp").astype(jnp.float32)
    mid_group = (gathered.astype(jnp.float32) + 0.5 * summed).astype(jnp.bfloat16)
    mid_rows = lax.dynamic_slice_in_dim(
        mid_group, lax.axis_index("tp") * tokens.shape[0], tokens.shape[0], 0
    )
    second_terms = down_terms(hidden_units(mid_group, norm_two, gate_two, up_two), down_two)
    summed_two = lax.psum_scatter(
        second_terms.astype(jnp.bfloat16), "tp", scatter_dimension=0, tiled=True
    ).astype(jnp.float32)
    return (mid_rows.astype(jnp.float32) + 0.5 * summed_two).astype(jnp.bfloat16)


def solution(mesh):
    return jax.shard_map(
        on_device,
        mesh=mesh,
        in_specs=(
            P(("fs", "tp"), None),
            P(),
            P("fs", "tp"),
            P("fs", "tp"),
            P("tp", "fs"),
            P(),
            P("fs", "tp"),
            P("fs", "tp"),
            P("tp", "fs"),
        ),
        out_specs=P(("fs", "tp"), None),
        check_vma=False,
    )
```

profile of v0, /device:TPU:1, one launch (start us, length us, event | category | flops | bytes accessed | tf_op | source)
XLA Modules:
  0.0 630.3 jit_solution(18163117887727268943)
XLA Ops:
  6.5 0.7 all-gather.8.cloned.1.call-update
  7.3 0.0 all-gather.10.cloned.1.call-start
  7.3 0.7 all-gather.10.cloned.1.call-update
  8.0 0.0 all-gather.12.cloned.1.call-start
  8.1 0.7 all-gather.12.cloned.1.call-update
  8.7 0.0 all-gather.14.cloned.1.call-start
  8.8 0.5 all-gather.14.cloned.1.call-update
  9.3 0.0 all-reduce.2.cloned.1.call-start
  9.4 24.6 %all-gather.8.cloned.1.call-done = bf16[512,2048]{1,0:T(8,128)(2,1)} async-done(((bf16[128,2048]{1,0:T(8,128)(2,1)}), bf16[512,2048]{1,0:T(8,128)(2,1)}) %all-gather.8.cloned.1.call-update) | async-done | bytes 2097168 | tf_op jit(solution)/shard_map/all_gather | solution.py:33
  33.9 2.1 fusion.3
  36.0 77.7 %all-gather.10.cloned.1.call-done = bf16[2048,1152]{1,0:T(8,128)(2,1)} async-done(((bf16[256,1152]{1,0:T(8,128)(2,1)}), bf16[2048,1152]{1,0:T(8,128)(2,1)}) %all-gather.10.cloned.1.call-update) | async-done | bytes 4718608 | tf_op jit(solution)/shard_map/all_gather | solution.py:18
  113.7 7.3 %fusion.11 = f32[512,1152]{1,0:T(8,128)} fusion(bf16[2048,1152]{1,0:T(8,128)(2,1)} %all-gather.10.cloned.1.call-done, bf16[512,2048]{1,0:T(8,128)(2,1)} %all-gather.8.cloned.1.call-done, f32[2048]{0:T(1024)S(1)} %copy-done.2, f32[512]{0:T(512)S(1)} %add_rsqrt_fusion.1), kind=kOutput, calls=%fused_computation.19 | convolution fusion | flops 2420113408 | bytes 9185280 | tf_op jit(solution)/shard_map/dot_general | solution.py:21
  121.0 72.6 %all-gather.12.cloned.1.call-done = bf16[2048,1152]{1,0:T(8,128)(2,1)} async-done(((bf16[256,1152]{1,0:T(8,128)(2,1)}), bf16[2048,1152]{1,0:T(8,128)(2,1)}) %all-gather.12.cloned.1.call-update) | async-done | bytes 4718608 | tf_op jit(solution)/shard_map/all_gather | solution.py:19
  193.6 81.5 %all-gather.14.cloned.1.call-done = bf16[1152,2048]{1,0:T(8,128)(2,1)} async-done(((bf16[1152,256]{1,0:T(8,128)(2,1)}), bf16[1152,2048]{1,0:T(8,128)(2,1)}) %all-gather.14.cloned.1.call-update) | async-done | bytes 4718608 | tf_op jit(solution)/shard_map/all_gather | solution.py:28
  275.1 12.2 %convolution_convert_fusion.1 = bf16[512,2048]{1,0:T(8,128)(2,1)} fusion(bf16[1152,2048]{1,0:T(8,128)(2,1)} %all-gather.14.cloned.1.call-done, bf16[2048,1152]{1,0:T(8,128)(2,1)} %all-gather.12.cloned.1.call-done, f32[512,1152]{1,0:T(8,128)} %fusion.11, bf16[512,2048]{1,0:T(8,128)(2,1)S(1)} %copy-done, f32[2048]{0:T(1024)S(1)} %copy-done.2, ...), kind=kOutput, calls=%fused_computation.17 | convolution fusion | flops 4840620032 | bytes 16001024 | tf_op jit(solution)/shard_map/dot_general | solution.py:27
  287.3 0.0 all-reduce.2.cloned.1.call-update
  287.3 0.0 all-gather.16.cloned.1.call-start
  287.4 0.5 all-gather.16.cloned.1.call-update
  287.9 0.0 all-gather.18.cloned.1.call-start
  287.9 0.7 all-gather.18.cloned.1.call-update
  288.7 0.0 all-gather.20.cloned.1.call-start
  288.7 0.7 all-gather.20.cloned.1.call-update
  289.4 0.2 reduce-scatter.2.cloned.1.call-start
  289.6 47.9 %all-reduce.2.cloned.1.call-done = bf16[512,2048]{1,0:T(8,128)(2,1)} async-done(((bf16[512,2048]{1,0:T(8,128)(2,1)}), bf16[512,2048]{1,0:T(8,128)(2,1)}) %all-reduce.2.cloned.1.call-update) | async-done | bytes 2097168 | tf_op jit(solution)/shard_map/psum | solution.py:35
  337.6 4.0 fusion
  341.6 76.3 %all-gather.16.cloned.1.call-done = bf16[2048,1152]{1,0:T(8,128)(2,1)} async-done(((bf16[256,1152]{1,0:T(8,128)(2,1)}), bf16[2048,1152]{1,0:T(8,128)(2,1)}) %all-gather.16.cloned.1.call-update) | async-done | bytes 4718608 | tf_op jit(solution)/shard_map/all_gather | solution.py:18
  417.9 7.4 %fusion.15 = f32[512,1152]{1,0:T(8,128)} fusion(bf16[2048,1152]{1,0:T(8,128)(2,1)} %all-gather.16.cloned.1.call-done, bf16[512,2048]{1,0:T(8,128)(2,1)} %get-tuple-element.6, f32[2048]{0:T(1024)S(1)} %copy-done.3, f32[512]{0:T(512)S(1)} %add_rsqrt_fusion), kind=kOutput, calls=%fused_computation.20 | convolution fusion | flops 2420113408 | bytes 9185280 | tf_op jit(solution)/shard_map/dot_general | solution.py:21
  425.3 72.5 %all-gather.18.cloned.1.call-done = bf16[2048,1152]{1,0:T(8,128)(2,1)} async-done(((bf16[256,1152]{1,0:T(8,128)(2,1)}), bf16[2048,1152]{1,0:T(8,128)(2,1)}) %all-gather.18.cloned.1.call-update) | async-done | bytes 4718608 | tf_op jit(solution)/shard_map/all_gather | solution.py:19
  497.8 81.7 %all-gather.20.cloned.1.call-done = bf16[1152,2048]{1,0:T(8,128)(2,1)} async-done(((bf16[1152,256]{1,0:T(8,128)(2,1)}), bf16[1152,2048]{1,0:T(8,128)(2,1)}) %all-gather.20.cloned.1.call-update) | async-done | bytes 4718608 | tf_op jit(solution)/shard_map/all_gather | solution.py:28
  579.5 12.1 %convolution_convert_fusion = bf16[512,2048]{1,0:T(8,128)(2,1)} fusion(bf16[1152,2048]{1,0:T(8,128)(2,1)} %all-gather.20.cloned.1.call-done, bf16[2048,1152]{1,0:T(8,128)(2,1)} %all-gather.18.cloned.1.call-done, f32[512,1152]{1,0:T(8,128)} %fusion.15, bf16[512,2048]{1,0:T(8,128)(2,1)S(1)} %copy-done.1, f32[2048]{0:T(1024)S(1)} %copy-done.3, ...), kind=kOutput, calls=%fused_computation.16 | convolution fusion | flops 4840620032 | bytes 16001024 | tf_op jit(solution)/shard_map/dot_general | solution.py:27
  591.6 30.1 %reduce-scatter.2.cloned.1.call-done = bf16[128,2048]{1,0:T(8,128)(2,1)} async-done(((bf16[512,2048]{1,0:T(8,128)(2,1)}), bf16[128,2048]{1,0:T(8,128)(2,1)}) %reduce-scatter.2.cloned.1.call-update) | async-done | bytes 524304 | tf_op jit(solution)/shard_map/reduce_scatter | solution.py:41
  621.7 2.0 add_convert_fusion
  (12 shorter events, 0.1 us)
Async XLA Ops:
  6.5 107.2 %copy-start.2 = (f32[2048]{0:T(1024)S(1)}, f32[2048]{0:T(1024)}, u32[]{:S(2)}) copy-start(f32[2048]{0:T(1024)} %param.10) | copy-start | bytes 24580
  6.5 27.4 %all-gather.8.cloned.1.call-start = ((), (), s32[]{:S(2)}) async-start(), calls=%async_computation.1 | async-start | bytes 2621440 | tf_op jit(solution)/shard_map/all_gather | solution.py:33
  7.3 106.4 %all-gather.10.cloned.1.call-start = ((), (), s32[]{:S(2)}) async-start(), calls=%async_computation.2 | async-start | bytes 5308416 | tf_op jit(solution)/shard_map/all_gather | solution.py:18
  8.0 185.6 %all-gather.12.cloned.1.call-start = ((), (), s32[]{:S(2)}) async-start(), calls=%async_computation.3 | async-start | bytes 5308416 | tf_op jit(solution)/shard_map/all_gather | solution.py:19
  8.7 266.4 %all-gather.14.cloned.1.call-start = ((), (), s32[]{:S(2)}) async-start(), calls=%async_computation.4 | async-start | bytes 5308416 | tf_op jit(solution)/shard_map/all_gather | solution.py:28
  9.3 328.2 %all-reduce.2.cloned.1.call-start = ((), (), s32[]{:S(2)}) async-start(), calls=%async_computation.5 | async-start | bytes 4194304 | tf_op jit(solution)/shard_map/psum | solution.py:35
  36.0 239.1 %copy-start = (bf16[512,2048]{1,0:T(8,128)(2,1)S(1)}, bf16[512,2048]{1,0:T(8,128)(2,1)}, u32[]{:S(2)}) copy-start(bf16[512,2048]{1,0:T(8,128)(2,1)} %all-gather.8.cloned.1.call-done) | copy-start | bytes 6291460
  287.3 130.6 %all-gather.16.cloned.1.call-start = ((), (), s32[]{:S(2)}) async-start(), calls=%async_computation.6 | async-start | bytes 5308416 | tf_op jit(solution)/shard_map/all_gather | solution.py:18
  287.9 209.9 %all-gather.18.cloned.1.call-start = ((), (), s32[]{:S(2)}) async-start(), calls=%async_computation.7 | async-start | bytes 5308416 | tf_op jit(solution)/shard_map/all_gather | solution.py:19
  288.7 290.8 %all-gather.20.cloned.1.call-start = ((), (), s32[]{:S(2)}) async-start(), calls=%async_computation.8 | async-start | bytes 5308416 | tf_op jit(solution)/shard_map/all_gather | solution.py:28
  289.4 128.5 %copy-start.3 = (f32[2048]{0:T(1024)S(1)}, f32[2048]{0:T(1024)}, u32[]{:S(2)}) copy-start(f32[2048]{0:T(1024)} %param.14) | copy-start | bytes 24580
  289.4 332.3 %reduce-scatter.2.cloned.1.call-start = ((), (), s32[]{:S(2)}) async-start(), calls=%async_computation.9 | async-start | bytes 2621440 | tf_op jit(solution)/shard_map/reduce_scatter | solution.py:41
  417.9 161.6 %copy-start.1 = (bf16[512,2048]{1,0:T(8,128)(2,1)S(1)}, bf16[512,2048]{1,0:T(8,128)(2,1)}, u32[]{:S(2)}) copy-start(bf16[512,2048]{1,0:T(8,128)(2,1)} %get-tuple-element.6) | copy-start | bytes 6291460
Sparse Core Ops, SparseCore 0:
  8.9 25.0 all-gather.7
  36.1 77.5 all-gather.9
  115.9 77.6 all-gather.11
  195.5 79.5 all-gather.13
  287.4 50.0 all-reduce.1
  339.6 78.2 all-gather.15
  420.1 77.6 all-gather.17
  499.8 79.5 all-gather.19
  591.8 29.9 reduce-scatter.1
where the time goes:
time: 631 us; the launch traced here: 630 us
  waiting for transfers between devices  569 us (90%)
  matrix products  39 us (6%)
  between operations  13.2 us (2%)
  other arithmetic  8.11 us (1%)
    all_gather x2, waiting for transfers between devices, down_terms(): lax.all_gather(down_w, 'fs', axis=1, tiled=True)  163 us
    all_gather x2, waiting for transfers between devices, hidden_units(): lax.all_gather(gate_w, 'fs', axis=0, tiled=True)  154 us
    all_gather x2, waiting for transfers between devices, hidden_units(): lax.all_gather(up_w, 'fs', axis=0, tiled=True)  145 us
    psum x1, waiting for transfers between devices, on_device(): lax.psum(first_terms.astype(jnp.bfloat16), 'tp').astype(jnp.float32)  47.9 us
    reduce_scatter x1, waiting for transfers between devices, on_device(): lax.psum_scatter(second_terms.astype(jnp.bfloat16), 'tp', scatter_dimensi...  30.1 us
    all_gather x1, waiting for transfers between devices, on_device(): gathered = lax.all_gather(tokens, 'tp', axis=0, tiled=True)  24.6 us
    dot_general x2, matrix products, down_terms(): jnp.dot(hidden, lax.all_gather(down_w, 'fs', axis=1, tiled=True), preferr...  24.3 us
    dot_general x2, matrix products, hidden_units(): gate_sum = jnp.dot(normed, gate_full, preferred_element_type=jnp.float32)  14.7 us
  transfers between devices with their start and end apart: 9, of which 9 were waited for; matrix products, arithmetic and copies ran while one was open for 3% of the time, Pallas kernels for 0%

commit v1 on v0

--- a/solution.py
+++ b/solution.py
@@ -1,9 +1,14 @@
+import functools
+
 import jax
 import jax.numpy as jnp
 from jax import lax
+from jax.experimental import pallas as pl
+from jax.experimental.pallas import tpu as pltpu
 from jax.sharding import PartitionSpec as P
 
 eps = 1e-06
+MESH = pl.DeviceIdType.MESH
 
 
 def normalize(rows, gain):
@@ -29,7 +34,7 @@
     )
 
 
-def on_device(tokens, norm_one, gate_one, up_one, down_one, norm_two, gate_two, up_two, down_two):
+def plain_on_device(tokens, norm_one, gate_one, up_one, down_one, norm_two, gate_two, up_two, down_two):
     gathered = lax.all_gather(tokens, "tp", axis=0, tiled=True)
     first_terms = down_terms(hidden_units(gathered, norm_one, gate_one, up_one), down_one)
     summed = lax.psum(first_terms.astype(jnp.bfloat16), "tp").astype(jnp.float32)
@@ -44,9 +49,357 @@
     return (mid_rows.astype(jnp.float32) + 0.5 * summed_two).astype(jnp.bfloat16)
 
 
+def kernel(
+    nz, n_tp,
+    tok_h, n1, g1_h, u1_h, d1_h, n2, g2_h, u2_h, d2_h,
+    out,
+    gu, dn, xs, mid, normed, gate, hidden, part, rs,
+    loc_sem, tok_sem, w_recv, z_send, y_send, x_send, x_recv, m_send, m_recv, rs_send, rs_recv,
+):
+    fs, tp = lax.axis_index("fs"), lax.axis_index("tp")
+    z, y = fs // 2, fs % 2
+    oy = 1 - y
+    n_fs = 2 * nz
+    hbm = [g1_h, u1_h, d1_h, g2_h, u2_h, d2_h]
+    n_w = len(hbm)
+    rows, dim = tok_h.shape
+    depth, width = g1_h.shape
+    cols = d1_h.shape[1]
+    gu_at = {0: 0, 1: 1, 3: 2, 4: 3}
+    dn_at = {2: 0, 5: 1}
+
+    gu_cut = depth - max(16, (depth * 3 // 16) // 16 * 16)
+    dn_cut = width - max(16, (width // 6) // 16 * 16)
+
+    def block(w, src):
+        return gu.at[gu_at[w], src] if w in gu_at else dn.at[dn_at[w], src]
+
+    def piece(w, src, p):
+        cut, full = (gu_cut, depth) if w in gu_at else (dn_cut, width)
+        return block(w, src).at[pl.ds(0, cut) if p == 0 else pl.ds(cut, full - cut)]
+
+    def locals_(w):
+        return pltpu.make_async_copy(hbm[w], block(w, fs), loc_sem.at[w])
+
+    def z_copy(w, p, src, up):
+        to = (z + 1 if up else z - 1) * 2 + y
+        return pltpu.make_async_remote_copy(
+            src_ref=piece(w, src, p), dst_ref=piece(w, src, p),
+            send_sem=z_send.at[w, p, src, 1 if up else 0], recv_sem=w_recv.at[w, p, src],
+            device_id=(to, tp), device_id_type=MESH)
+
+    def y_copy(w, p, src):
+        return pltpu.make_async_remote_copy(
+            src_ref=piece(w, src, p), dst_ref=piece(w, src, p),
+            send_sem=y_send.at[w, p, src // 2], recv_sem=w_recv.at[w, p, src],
+            device_id=(z * 2 + oy, tp), device_id_type=MESH)
+
+    def arrived(w, p, src):
+        ref = piece(w, src, p)
+        pltpu.make_async_copy(ref, ref, w_recv.at[w, p, src]).wait()
+
+    def both_z(w, p, src):
+        @pl.when(z < nz - 1)
+        def _():
+            z_copy(w, p, src, True).start()
+
+        @pl.when(z > 0)
+        def _():
+            z_copy(w, p, src, False).start()
+
+    def own_start(w):
+        locals_(w).wait()
+        y_copy(w, 1, fs).start()
+        both_z(w, 0, fs)
+        y_copy(w, 0, fs).start()
+        both_z(w, 1, fs)
+
+    def cross(w):
+        src = z * 2 + oy
+        arrived(w, 1, src)
+        both_z(w, 1, src)
+
+    def relay(w, d):
+        def one(sz, going_up, more):
+            own, other = sz * 2 + y, sz * 2 + oy
+            for p, src in ((0, own), (1, own), (1, other)):
+                arrived(w, p, src)
+
+                @pl.when(more)
+                def _():
+                    z_copy(w, p, src, going_up).start()
+                if p == 0:
+                    y_copy(w, p, src).start()
+
+        @pl.when(z - d >= 0)
+        def _():
+            one(z - d, True, z < nz - 1)
+
+        @pl.when(z + d < nz)
+        def _():
+            one(z + d, False, z > 0)
+
+    def at_distance(d, do):
+        if d == 0:
+            do(z)
+        else:
+            @pl.when(z - d >= 0)
+            def _():
+                do(z - d)
+
+            @pl.when(z + d < nz)
+            def _():
+                do(z + d)
+
+    def wait_other(w, d):
+        at_distance(d, lambda sz: arrived(w, 0, sz * 2 + oy))
+
+    def peer(j):
+        return lax.rem(tp + j, n_tp)
+
+    def x_copy(j):
+        return pltpu.make_async_remote_copy(
+            src_ref=xs.at[tp], dst_ref=xs.at[tp], send_sem=x_send.at[j], recv_sem=x_recv.at[tp],
+            device_id=(fs, peer(j)), device_id_type=MESH)
+
+    def m_copy(j):
+        return pltpu.make_async_remote_copy(
+            src_ref=mid.at[tp], dst_ref=mid.at[tp], send_sem=m_send.at[j], recv_sem=m_recv.at[tp],
+            device_id=(fs, peer(j)), device_id_type=MESH)
+
+    def rs_copy(h, j, src):
+        return pltpu.make_async_remote_copy(
+            src_ref=part.at[h, peer(j), src], dst_ref=rs.at[h, tp, src],
+            send_sem=rs_send.at[h, j, src], recv_sem=rs_recv.at[h, tp, src],
+            device_id=(fs, peer(j)), device_id_type=MESH)
+
+    def norm_all(source, gain):
+        @pl.loop(0, n_tp)
+        def _(t):
+            normed[pl.ds(pl.multiple_of(t * rows, rows), rows), :] = normalize(source[t], gain[...])
+
+    step_cols = next(c for c in (384, 256, 128) if width % c == 0)
+
+    def project(w, finish):
+        at = gu_at[w]
+
+        @pl.loop(0, width // step_cols)
+        def _(i):
+            c = pl.ds(pl.multiple_of(i * step_cols, step_cols), step_cols)
+            weights = gu[at, :, :, c].reshape(dim, step_cols)
+            finish(c, jnp.dot(normed[...], weights, preferred_element_type=jnp.float32))
+
+    def keep_gate(c, value):
+        gate[:, c] = value
+
+    def keep_hidden(c, value):
+        g = gate[:, c]
+        hidden[:, c] = (g / (1.0 + jnp.exp(-g)) * value).astype(jnp.bfloat16)
+
+    def down_block(h, src):
+        value = jnp.dot(hidden[...], dn[h, src], preferred_element_type=jnp.float32).astype(jnp.bfloat16)
+        for t in range(n_tp):
+            part[h, t, src] = value[t * rows:(t + 1) * rows]
+
+    def rs_start(h, src):
+        for j in range(1, n_tp):
+            rs_copy(h, j, src).start()
+
+    def finish(h, base, store):
+        @pl.loop(0, n_fs)
+        def _(src):
+            total = part[h, tp, src].astype(jnp.float32)
+            for j in range(1, n_tp):
+                ref = rs.at[h, peer(j), src]
+                pltpu.make_async_copy(ref, ref, rs_recv.at[h, peer(j), src]).wait()
+                total = total + rs[h, peer(j), src].astype(jnp.float32)
+            c = pl.ds(pl.multiple_of(src * cols, cols), cols)
+            store(c, (base[tp, :, c].astype(jnp.float32) + 0.5 * total).astype(jnp.bfloat16))
+
+    tok_local = pltpu.make_async_copy(tok_h, xs.at[tp], tok_sem)
+    locals_(0).start()
+    tok_local.start()
+    for w in range(1, n_w):
+        locals_(w).start()
+    barrier = pltpu.get_barrier_semaphore()
+    pl.semaphore_signal(barrier, inc=1, device_id=(z * 2 + oy, tp), device_id_type=MESH)
+    for j in range(1, n_tp):
+        pl.semaphore_signal(barrier, inc=1, device_id=(fs, peer(j)), device_id_type=MESH)
+
+    @pl.when(z < nz - 1)
+    def _():
+        pl.semaphore_signal(barrier, inc=1, device_id=((z + 1) * 2 + y, tp), device_id_type=MESH)
+
+    @pl.when(z > 0)
+    def _():
+        pl.semaphore_signal(barrier, inc=1, device_id=((z - 1) * 2 + y, tp), device_id_type=MESH)
+
+    neighbours = (z + nz - 1) // nz + (2 * nz - 2 - z) // nz
+    pl.semaphore_wait(barrier, n_tp + neighbours)
+
+    own_start(0)
+    tok_local.wait()
+    for j in range(1, n_tp):
+        x_copy(j).start()
+
+    def wait_mid():
+        for j in range(1, n_tp):
+            ref = mid.at[peer(j)]
+            pltpu.make_async_copy(ref, ref, m_recv.at[peer(j)]).wait()
+
+    def compute(w):
+        if w == 0:
+            for j in range(1, n_tp):
+                ref = xs.at[peer(j)]
+                pltpu.make_async_copy(ref, ref, x_recv.at[peer(j)]).wait()
+            norm_all(xs, n1)
+            project(w, keep_gate)
+        elif w == 3:
+            wait_mid()
+            norm_all(mid, n2)
+            project(w, keep_gate)
+        elif w in (1, 4):
+            project(w, keep_hidden)
+        elif w == 2:
+            @pl.loop(0, n_fs)
+            def _(src):
+                down_block(0, src)
+                rs_start(0, src)
+
+    def down_own(d):
+        def do(sz):
+            down_block(1, sz * 2 + y)
+            rs_start(1, sz * 2 + y)
+        at_distance(d, do)
+
+    def down_other(d):
+        def do(sz):
+            arrived(5, 0, sz * 2 + oy)
+            down_block(1, sz * 2 + oy)
+            rs_start(1, sz * 2 + oy)
+        at_distance(d, do)
+
+    def full(w):
+        for d in range(nz):
+            wait_other(w, d)
+        compute(w)
+
+    last = n_w - 1
+
+    def store_mid(c, value):
+        mid[tp, :, c] = value
+
+    def store_out(c, value):
+        out[:, c] = value
+
+    for s in range(n_w + nz - 2):
+        if s + 1 < n_w:
+            own_start(s + 1)
+        if s == 3 + nz:
+            finish(0, xs, store_mid)
+            for j in range(1, n_tp):
+                m_copy(j).start()
+        for d in range(nz - 1, 0, -1):
+            if 0 <= s - d < n_w:
+                relay(s - d, d)
+        if s < n_w:
+            cross(s)
+        if 0 <= s - nz < n_w:
+            full(s - nz)
+    full(last - 1)
+    for d in range(nz - 1):
+        down_own(d)
+        if d < nz - 2:
+            down_other(d)
+    relay(last, nz - 1)
+    down_own(nz - 1)
+    down_other(nz - 2)
+    down_other(nz - 1)
+    finish(1, mid, store_out)
+
+    def sent_z(w, p, src, up):
+        pltpu.make_async_copy(piece(w, src, p), piece(w, src, p), z_send.at[w, p, src, 1 if up else 0]).wait()
+
+    for w in range(n_w):
+        for p in range(2):
+            for sz in range(nz):
+                if p == 0:
+                    ref = piece(w, sz * 2 + y, 0)
+                    pltpu.make_async_copy(ref, ref, y_send.at[w, 0, sz]).wait()
+                for sy in ((y,) if p == 0 else (y, oy)):
+                    src = sz * 2 + sy
+
+                    @pl.when((z >= sz) & (z < nz - 1))
+                    def _():
+                        sent_z(w, p, src, True)
+
+                    @pl.when((z <= sz) & (z > 0))
+                    def _():
+                        sent_z(w, p, src, False)
+        ref = piece(w, fs, 1)
+        pltpu.make_async_copy(ref, ref, y_send.at[w, 1, z]).wait()
+    for j in range(1, n_tp):
+        x_copy(j).wait_send()
+        m_copy(j).wait_send()
+
+        @pl.loop(0, n_fs)
+        def _(src):
+            for h in range(2):
+                rs_copy(h, j, src).wait_send()
+
+
+def line_on_device(nz, n_tp, tokens, norm_one, gate_one, up_one, down_one, norm_two, gate_two, up_two, down_two):
+    rows, dim = tokens.shape
+    depth, width = gate_one.shape
+    cols = down_one.shape[1]
+    n_fs, group = 2 * nz, n_tp * rows
+    bf, f32 = jnp.bfloat16, jnp.float32
+    hbm, vmem = pl.BlockSpec(memory_space=pl.ANY), pl.BlockSpec(memory_space=pltpu.VMEM)
+    dma = pltpu.SemaphoreType.DMA
+    return pl.pallas_call(
+        functools.partial(kernel, nz, n_tp),
+        out_shape=jax.ShapeDtypeStruct((rows, dim), bf),
+        in_specs=[hbm, vmem, hbm, hbm, hbm, vmem, hbm, hbm, hbm],
+        out_specs=vmem,
+        scratch_shapes=[
+            pltpu.VMEM((4, n_fs, depth, width), bf),
+            pltpu.VMEM((2, n_fs, width, cols), bf),
+            pltpu.VMEM((n_tp, rows, dim), bf),
+            pltpu.VMEM((n_tp, rows, dim), bf),
+            pltpu.VMEM((group, dim), bf),
+            pltpu.VMEM((group, width), f32),
+            pltpu.VMEM((group, width), bf),
+            pltpu.VMEM((2, n_tp, n_fs, rows, cols), bf),
+            pltpu.VMEM((2, n_tp, n_fs, rows, cols), bf),
+            dma((6,)), dma,
+            dma((6, 2, n_fs)), dma((6, 2, n_fs, 2)), dma((6, 2, nz)),
+            dma((n_tp,)), dma((n_tp,)), dma((n_tp,)), dma((n_tp,)),
+            dma((2, n_tp, n_fs)), dma((2, n_tp, n_fs)),
+        ],
+        compiler_params=pltpu.CompilerParams(
+            collective_id=0, has_side_effects=True, vmem_limit_bytes=66_000_000
+        ),
+    )(tokens, norm_one.reshape(1, -1), gate_one, up_one, down_one,
+      norm_two.reshape(1, -1), gate_two, up_two, down_two)
+
+
+def pairs_along_y(mesh):
+    line = [d.coords for d in mesh.devices[:, 0]]
+    if len(line) % 2 or len(line) < 6:
+        return False
+    nz = len(line) // 2
+    return all(
+        line[2 * k][2] == line[2 * k + 1][2] == line[0][2] + k
+        and line[2 * k + 1][1] == line[2 * k][1] + 1 == line[0][1] + 1
+        for k in range(nz)
+    )
+
+
 def solution(mesh):
+    n_fs, n_tp = mesh.shape["fs"], mesh.shape["tp"]
+    body = functools.partial(line_on_device, n_fs // 2, n_tp) if pairs_along_y(mesh) else plain_on_device
     return jax.shard_map(
-        on_device,
+        body,
         mesh=mesh,
         in_specs=(
             P(("fs", "tp"), None),

time: 631 us -> 309 us (0.49)
  waiting for transfers between devices: 569 us -> 0 us
  Pallas kernels: 0 us -> 307 us
  matrix products: 39 us -> 0 us
  between operations: 13.2 us -> 0.01 us
  other arithmetic: 8.11 us -> 0 us
    all_gather x7 -> x0, waiting for transfers between devices: 487 us -> none  [the longest x2 163 us: down_terms(): lax.all_gather(down_w, 'fs', axis=1, tiled=True)]
    pallas_call x0 -> x1, Pallas kernels: none -> 307 us  [line_on_device(): pl.pallas_call(functools.partial(kernel, nz, n_tp), out_shape=jax.ShapeDt...]
    psum x1 -> x0, waiting for transfers between devices: 47.9 us -> none  [on_device(): lax.psum(first_terms.astype(jnp.bfloat16), 'tp').astype(jnp.float32)]
    dot_general x4 -> x0, matrix products: 39 us -> none  [the longest x2 24.3 us: down_terms(): jnp.dot(hidden, lax.all_gather(down_w, 'fs', axis=1, tiled=True), preferr...]
    reduce_scatter x1 -> x0, waiting for transfers between devices: 30.1 us -> none  [on_device(): lax.psum_scatter(second_terms.astype(jnp.bfloat16), 'tp', scatter_dimensi...]
  transfers between devices with their start and end apart: 9 -> 0, of which waited for: 9 -> 0; matrix products, arithmetic and copies ran while one was open for 3% -> 0% of each run, Pallas kernels for 0% -> 0%
where the time goes in v1:
time: 309 us
  Pallas kernels  307 us (99%)
    pallas_call x1, Pallas kernels, line_on_device(): pl.pallas_call(functools.partial(kernel, nz, n_tp), out_shape=jax.ShapeDt...  307 us

profile of v1, /device:TPU:1, one launch (start us, length us, event | category | flops | bytes accessed | tf_op | source)
XLA Modules:
  0.0 309.0 jit_solution(11711745281926315926)
XLA Ops:
  0.0 307.1 %shard_map.91 = bf16[128,2048]{1,0:T(8,128)(2,1)} custom-call(bf16[128,2048]{1,0:T(8,128)(2,1)} %tok_h.1, f32[1,2048]{1,0:T(1,128)} %bitcast.2, bf16[256,1152]{1,0:T(8,128)(2,1)} %g1_h.1, bf16[256,1152]{1,0:T(8,128)(2,1)} %u1_h.1, bf16[1152,256]{1,0:T(8,128)(2,1)} %d1_h.1, f32[1,2048]{1,0:T(1,128)} %bitcast.3, bf16[256,1152]{1,0:T(8,128)(2,1)} %g2_h.1, ...), custom_call_target="tpu_custom_call" | custom-call | tf_op jit(solution)/shard_map/pallas_call | solution.py:359
  307.1 1.9 copy.11

commit v2 on v1

--- a/solution.py
+++ b/solution.py
@@ -68,14 +68,17 @@
     gu_at = {0: 0, 1: 1, 3: 2, 4: 3}
     dn_at = {2: 0, 5: 1}
 
-    gu_cut = depth - max(16, (depth * 3 // 16) // 16 * 16)
-    dn_cut = width - max(16, (width // 6) // 16 * 16)
+    shares = (2, 2, 2, 2, 3, 3)
+
+    def cut_of(w, full):
+        return full - max(16, full * shares[w] // 256 * 16)
 
     def block(w, src):
         return gu.at[gu_at[w], src] if w in gu_at else dn.at[dn_at[w], src]
 
     def piece(w, src, p):
-        cut, full = (gu_cut, depth) if w in gu_at else (dn_cut, width)
+        full = depth if w in gu_at else width
+        cut = cut_of(w, full)
         return block(w, src).at[pl.ds(0, cut) if p == 0 else pl.ds(cut, full - cut)]
 
     def locals_(w):
@@ -292,21 +295,25 @@
     def store_out(c, value):
         out[:, c] = value
 
+    for w in range(1, 2):
+        own_start(w)
     for s in range(n_w + nz - 2):
-        if s + 1 < n_w:
-            own_start(s + 1)
-        if s == 3 + nz:
-            finish(0, xs, store_mid)
-            for j in range(1, n_tp):
-                m_copy(j).start()
+        if s + 2 < n_w:
+            own_start(s + 2)
         for d in range(nz - 1, 0, -1):
             if 0 <= s - d < n_w:
                 relay(s - d, d)
         if s < n_w:
             cross(s)
-        if 0 <= s - nz < n_w:
-            full(s - nz)
-    full(last - 1)
+        if s == 2 + nz:
+            finish(0, xs, store_mid)
+            for j in range(1, n_tp):
+                m_copy(j).start()
+        elif s == 3 + nz:
+            full(3)
+            full(4)
+        elif 0 <= s - nz + 1 < n_w:
+            full(s - nz + 1)
     for d in range(nz - 1):
         down_own(d)
         if d < nz - 2:

time: 309 us -> 291 us (0.942)
  Pallas kernels: 307 us -> 289 us
    pallas_call x1, Pallas kernels: 307 us -> 289 us  [line_on_device(): pl.pallas_call(functools.partial(kernel, nz, n_tp), out_shape=jax.ShapeDt...]
where the time goes in v2:
time: 291 us
  Pallas kernels  289 us (99%)
    pallas_call x1, Pallas kernels, line_on_device(): pl.pallas_call(functools.partial(kernel, nz, n_tp), out_shape=jax.ShapeDt...  289 us

profile of v2, /device:TPU:1, one launch (start us, length us, event | category | flops | bytes accessed | tf_op | source)
XLA Modules:
  0.0 291.2 jit_solution(14520942383274981055)
XLA Ops:
  0.0 289.3 %shard_map.91 = bf16[128,2048]{1,0:T(8,128)(2,1)} custom-call(bf16[128,2048]{1,0:T(8,128)(2,1)} %tok_h.1, f32[1,2048]{1,0:T(1,128)} %bitcast.2, bf16[256,1152]{1,0:T(8,128)(2,1)} %g1_h.1, bf16[256,1152]{1,0:T(8,128)(2,1)} %u1_h.1, bf16[1152,256]{1,0:T(8,128)(2,1)} %d1_h.1, f32[1,2048]{1,0:T(1,128)} %bitcast.3, bf16[256,1152]{1,0:T(8,128)(2,1)} %g2_h.1, ...), custom_call_target="tpu_custom_call" | custom-call | tf_op jit(solution)/shard_map/pallas_call | solution.py:366
  289.4 1.9 copy.11
